TPU v7x, 32 devices: a whole 2x2x4 slice. The times are simulated.
32 devices in a mesh: sp: 4 (over z), fs: 4 (over y, x), tp: 2 (over core).
Axes of the slice: x: 2, y: 2, z: 4, core: 2. Of those that a mesh axis runs over, the one named last changes fastest.
Arguments:
- tokens: bfloat16 [4, 512, 4096], P('fs', 'sp'), may hold values from -6 to 6
- norm_gain: float32 [4096], replicated, may hold values from 0.1 to 1.9
- pool_proj: bfloat16 [4096, 1024], P(('sp', 'fs'), 'tp'), may hold values from -0.09375 to 0.09375
- query_proj: bfloat16 [4096, 1024], P(('sp', 'fs'), 'tp'), may hold values from -0.09375 to 0.09375
- key_proj: bfloat16 [4096, 1024], P(('sp', 'fs'), 'tp'), may hold values from -0.09375 to 0.09375
- value_proj: bfloat16 [4096, 1024], P(('sp', 'fs'), 'tp'), may hold values from -0.09375 to 0.09375
- pool_map: bfloat16 [4, 256, 256], replicated, may hold values from -0.375 to 0.375
- pool_scale: float32 [1024], replicated, may hold values from 0.1 to 1.9
- decay_rate: float32 [4], P('tp'), may hold values from 2e-05 to 0.034
- start_state: float32 [4, 4, 256, 256], P('fs', 'tp', 'sp'), may hold values from -96 to 96
- pool_back: bfloat16 [1024, 4096], P('tp', ('sp', 'fs')), may hold values from -0.125 to 0.125
- retention_back: bfloat16 [1024, 4096], P('tp', ('sp', 'fs')), may hold values from -0.125 to 0.125
Outputs:
- mixed: bfloat16 [4, 512, 4096], P('fs', ('sp', 'tp'))
All inputs are finite; a program needn't handle non-finite values.
Results may differ from a plain program's by a relative error of at most 0.014.
Values may be sent and summed in bfloat16 or wider, within the bound.
A program may use at most 128 MiB of HBM per device.

v0:
```python
import jax
import jax.numpy as jnp
from jax import lax
from jax.sharding import PartitionSpec as P

GROUPS = 4
BLOCK = 128
HALO = 16
eps = 1e-06
rope_base = 10000.0
highest_precision = lax.Precision.HIGHEST
window_list = (2, 4, 8, 16)


def shortened(x):
    return jax.tree.map(lambda a: a.astype(jnp.bfloat16) if a.dtype == jnp.float32 else a, x)


def shifted(x, axis, by):
    devices = lax.axis_size(axis)
    pairs = [(i, i + by) for i in range(devices) if 0 <= i + by < devices]
    return lax.ppermute(x, axis, pairs)


def carried_in(value, axis, join, neutral):
    count, mine = (lax.axis_size(axis), lax.axis_index(axis))
    pieces = jax.tree.map(lambda part: lax.all_gather(part, axis), value)
    running = jax.tree.map(
        lambda part, zero: jnp.full_like(part, 0) + jnp.asarray(zero, part.dtype), value, neutral
    )

    def turn(position, running):
        longer = join(running, jax.tree.map(lambda part: part[position], pieces))
        return jax.tree.map(lambda new, old: jnp.where(position < mine, new, old), longer, running)

    return lax.fori_loop(0, count - 1, turn, running)


def rotate(values, positions):
    half_dim = values.shape[-1] // 2
    inv_freq = 1.0 / rope_base ** jnp.linspace(0.0, 1.0, half_dim, dtype=jnp.float32)
    angles = positions.astype(jnp.float32)[:, None] * inv_freq[None, :]
    cosine = jnp.cos(angles)[:, None, :]
    sine = jnp.sin(angles)[:, None, :]
    first_half = values[..., :half_dim]
    second_half = values[..., half_dim:]
    return jnp.concatenate(
        [first_half * cosine - second_half * sine, first_half * sine + second_half * cosine],
        axis=-1,
    )


def trailing_sums(extended, length):
    begin = extended.shape[0] - length
    running = extended[begin:]
    results = []
    for behind in range(1, 16):
        running = running + extended[begin - behind : begin - behind + length]
        if behind + 1 in window_list:
            results.append(running)
    return results


def reshape_blocks(array):
    return array.reshape((array.shape[0] // BLOCK, BLOCK) + array.shape[1:])


def block_retention(queries, keys_in, values_in, decay_rate, initial):
    length, head_count, head_dim = queries.shape
    within = jnp.arange(BLOCK, dtype=jnp.float32)
    distance = within[:, None] - within[None, :]
    decay_mask = jnp.where(
        distance[None] >= 0,
        jnp.exp(-jnp.maximum(distance, 0.0)[None] * decay_rate[:, None, None]),
        0.0,
    )
    query_decay_factor = jnp.exp(-(within + 1.0)[:, None] * decay_rate[None, :])
    key_decay_factor = jnp.exp(-(BLOCK - 1.0 - within)[:, None] * decay_rate[None, :])
    block_decay_factor = jnp.exp(-BLOCK * decay_rate)

    def advance(state_carry, inputs):
        block_queries, block_keys, block_values = inputs
        scores = (
            jnp.einsum("ihk,jhk->hij", block_queries, block_keys, precision=highest_precision)
            * decay_mask
        )
        inside = jnp.einsum("hij,jhv->ihv", scores, block_values, precision=highest_precision)
        across_blocks = jnp.einsum(
            "bzy,zyx->bzx",
            block_queries * query_decay_factor[:, :, None],
            state_carry,
            precision=highest_precision,
        )
        state_carry = state_carry * block_decay_factor[:, None, None] + jnp.einsum(
            "flm,fld->lmd",
            block_keys * key_decay_factor[:, :, None],
            block_values,
            precision=highest_precision,
        )
        return (state_carry, inside + across_blocks)

    final_state, outputs = lax.scan(
        advance,
        initial,
        (reshape_blocks(queries), reshape_blocks(keys_in), reshape_blocks(values_in)),
    )
    return (outputs.reshape(length, head_count, values_in.shape[-1]), final_state)


def combine_states(earlier, latter):
    return (earlier[0] * latter[0], latter[0][:, None, None] * earlier[1] + latter[1])


def on_device(
    tokens,
    norm_gain,
    pool_proj,
    query_proj,
    key_proj,
    value_proj,
    pool_map,
    pool_scale,
    decay_rate,
    start_state,
    pool_back,
    retention_back,
):
    sequence = tokens[0]
    length = sequence.shape[0]
    tp_index = lax.axis_index("tp")
    sp_index = lax.axis_index("sp")
    tp_count = lax.axis_size("tp")
    floats = sequence.astype(jnp.float32)
    normed = (
        floats * lax.rsqrt(jnp.mean(floats * floats, axis=-1, keepdims=True) + eps) * norm_gain
    ).astype(jnp.bfloat16)
    group_normed = lax.all_gather(normed, "fs", axis=0, tiled=True)
    quarters = (
        lax.all_to_all(pool_proj, "fs", split_axis=1, concat_axis=0, tiled=True),
        lax.all_to_all(query_proj, "fs", split_axis=1, concat_axis=0, tiled=True),
        lax.all_to_all(key_proj, "fs", split_axis=1, concat_axis=0, tiled=True),
        lax.all_to_all(value_proj, "fs", split_axis=1, concat_axis=0, tiled=True),
    )
    pieces = (
        lax.all_gather(quarters[0], "sp", axis=0, tiled=True),
        lax.all_gather(quarters[1], "sp", axis=0, tiled=True),
        lax.all_gather(quarters[2], "sp", axis=0, tiled=True),
        lax.all_gather(quarters[3], "sp", axis=0, tiled=True),
    )
    partial_cols = tuple(
        (jnp.dot(group_normed, piece_w, preferred_element_type=jnp.float32) for piece_w in pieces)
    )
    rounded = tuple((result.astype(jnp.bfloat16) for result in partial_cols))
    pool_in, query_bf, key_bf, value_bf = jax.tree.map(
        lambda part, own: part.astype(own.dtype),
        lax.all_to_all(shortened(rounded), "fs", split_axis=0, concat_axis=1, tiled=True),
        rounded,
    )
    positions = jnp.arange(length, dtype=jnp.int32) + sp_index * length
    before = shifted(pool_in[length - HALO :], "sp", 1)
    extended = jnp.concatenate([before, pool_in], axis=0).astype(jnp.float32)
    stacked = jnp.stack(trailing_sums(extended, length))
    local_groups = GROUPS // tp_count
    channels = pool_in.shape[1]
    group_dim = channels // local_groups
    group_maps = lax.dynamic_slice_in_dim(pool_map, tp_index * local_groups, local_groups, 0)
    scales = lax.dynamic_slice_in_dim(pool_scale, tp_index * channels, channels, 0)
    windows = jnp.array(window_list, dtype=jnp.int32)
    pieces = []
    for group_idx in range(local_groups):
        chosen_group = tp_index * local_groups + group_idx
        lower = group_idx * group_dim
        chosen = lax.dynamic_index_in_dim(stacked, chosen_group, 0, keepdims=False)[
            :, lower : lower + group_dim
        ]
        counts = jnp.minimum(windows[chosen_group], positions + 1).astype(jnp.float32)
        inputs = extended[HALO:, lower : lower + group_dim]
        differ = (chosen / counts[:, None] - inputs).astype(jnp.bfloat16)
        pieces.append(jnp.dot(differ, group_maps[group_idx], preferred_element_type=jnp.float32))
    pool_out = (jnp.concatenate(pieces, axis=1) * scales).astype(jnp.bfloat16)
    head_count = decay_rate.shape[0]
    head_dim = query_bf.shape[1] // head_count
    queries = rotate(query_bf.astype(jnp.float32).reshape(length, head_count, head_dim), positions)
    keys_in = rotate(
        key_bf.astype(jnp.float32).reshape(length, head_count, head_dim), positions
    ) * head_dim ** (-0.5)
    values_in = value_bf.astype(jnp.float32).reshape(length, head_count, head_dim)
    zeros_state = jnp.zeros((head_count, head_dim, head_dim), jnp.float32)
    local_output, local_state = block_retention(
        queries, keys_in, values_in, decay_rate, zeros_state
    )
    span_decay = jnp.exp(-decay_rate * length)
    whole_start = lax.all_gather(start_state, "sp", axis=2, tiled=True)[0]
    span_factor, carried_over = carried_in(
        (span_decay, local_state), "sp", combine_states, (jnp.ones_like(span_decay), zeros_state)
    )
    offset_float = (sp_index * length).astype(jnp.float32)
    carried_over = carried_over + jnp.exp(-decay_rate * offset_float)[:, None, None] * whole_start
    steps_in = jnp.arange(length, dtype=jnp.float32) + 1.0
    query_rows_scaled = queries * jnp.exp(-steps_in[:, None] * decay_rate[None, :])[:, :, None]
    retained_output = local_output + jnp.einsum(
        "lpi,pib->lpb", query_rows_scaled, carried_over, precision=highest_precision
    )
    retained_output = retained_output * lax.rsqrt(
        jnp.mean(retained_output * retained_output, axis=-1, keepdims=True) + eps
    )
    ret_out = retained_output.reshape(length, head_count * head_dim).astype(jnp.bfloat16)
    pool_cols, retention_cols = (
        lax.all_gather(pool_back, ("sp", "fs"), axis=1, tiled=True),
        lax.all_gather(retention_back, ("sp", "fs"), axis=1, tiled=True),
    )
    weight_local = jnp.concatenate([pool_cols, retention_cols], axis=0)
    joined = jnp.concatenate([pool_out, ret_out], axis=1)
    mixed = lax.psum_scatter(
        jnp.dot(joined, weight_local, preferred_element_type=jnp.float32).astype(jnp.bfloat16),
        "tp",
        scatter_dimension=0,
        tiled=True,
    )
    return mixed[None]


def solution(mesh):
    placed = (
        P("fs", "sp", None),
        P(),
        P(("sp", "fs"), "tp"),
        P(("sp", "fs"), "tp"),
        P(("sp", "fs"), "tp"),
        P(("sp", "fs"), "tp"),
        P(),
        P(),
        P("tp"),
        P("fs", "tp", "sp", None),
        P("tp", ("sp", "fs")),
        P("tp", ("sp", "fs")),
    )
    return jax.shard_map(
        on_device,
        mesh=mesh,
        in_specs=placed,
        out_specs=P("fs", ("sp", "tp"), None),
        check_vma=False,
    )
```

profile of v0, /device:TPU:0, one launch (start us, length us, event | category | flops | bytes accessed | tf_op | source)
XLA Modules:
  0.0 432.0 jit_solution(100196734017617633)
XLA Ops:
  6.5 1.2 copy.58
  7.7 10.7 %all_to_all.137 = bf16[256,4,128]{0,2,1:T(8,128)(2,1)S(1)} all-to-all(bf16[256,4,128]{0,2,1:T(8,128)(2,1)S(1)} %bitcast.100), channel_id=1, replica_groups=mesh['sp'=4,'fs'=4,'tp'=2] {'fs'}, dimensions={1} | all-to-all | bytes 524288 | tf_op jit(solution)/shard_map/all_to_all | solution.py:140
  18.4 0.9 copy.59
  19.4 1.5 fusion.8
  20.9 2.6 fusion.10
  23.7 8.1 %all_to_all.138 = bf16[256,4,128]{0,2,1:T(8,128)(2,1)S(1)} all-to-all(bf16[256,4,128]{0,2,1:T(8,128)(2,1)S(1)} %bitcast.101), channel_id=1, replica_groups=mesh['sp'=4,'fs'=4,'tp'=2] {'fs'}, dimensions={1} | all-to-all | bytes 524288 | tf_op jit(solution)/shard_map/all_to_all | solution.py:141
  31.9 0.8 copy.64
  32.9 8.1 %all_to_all.139 = bf16[256,4,128]{0,2,1:T(8,128)(2,1)S(1)} all-to-all(bf16[256,4,128]{0,2,1:T(8,128)(2,1)S(1)} %bitcast.102), channel_id=1, replica_groups=mesh['sp'=4,'fs'=4,'tp'=2] {'fs'}, dimensions={1} | all-to-all | bytes 524288 | tf_op jit(solution)/shard_map/all_to_all | solution.py:142
  41.0 0.8 copy.56
  41.9 0.8 copy.50
  42.8 3.4 all-to-all-start
  48.0 3.5 all-to-all-done
  51.5 0.9 copy.51
  52.4 48.6 %all-gather.11.cloned.1.call-done = bf16[512,4096]{1,0:T(8,128)(2,1)} async-done(((bf16[128,4096]{1,0:T(8,128)(2,1)}), bf16[512,4096]{1,0:T(8,128)(2,1)}) %all-gather.11.cloned.1.call-update) | async-done | bytes 4194320 | tf_op jit(solution)/shard_map/all_gather | solution.py:137
  101.0 3.7 convolution_convert_fusion.1
  104.7 0.8 copy.60
  105.5 3.3 all-to-all-start.5
  108.8 21.8 %all-gather.19.cloned.1.call-done = bf16[4096,128]{1,0:T(8,128)(2,1)} async-done(((bf16[1024,128]{1,0:T(8,128)(2,1)}), bf16[4096,128]{1,0:T(8,128)(2,1)}) %all-gather.19.cloned.1.call-update) | async-done | bytes 1048592 | tf_op jit(solution)/shard_map/all_gather | solution.py:147
  130.6 3.7 convolution_convert_fusion
  134.3 0.8 copy.65
  135.1 3.7 all-to-all-start.7
  138.7 20.7 %all-gather.15.cloned.1.call-done = bf16[4096,128]{1,0:T(8,128)(2,1)} async-done(((bf16[1024,128]{1,0:T(8,128)(2,1)}), bf16[4096,128]{1,0:T(8,128)(2,1)}) %all-gather.15.cloned.1.call-update) | async-done | bytes 1048592 | tf_op jit(solution)/shard_map/all_gather | solution.py:148
  159.4 4.4 %convolution_convert_fusion.2 = bf16[512,128]{1,0:T(8,128)(2,1)} fusion(bf16[512,4096]{1,0:T(8,128)(2,1)} %all-gather.11.cloned.1.call-done, bf16[4096,128]{1,0:T(8,128)(2,1)} %all-gather.15.cloned.1.call-done), kind=kOutput, calls=%fused_computation.19 | convolution fusion | flops 536936448 | bytes 5373952 | tf_op jit(solution)/shard_map/dot_general | solution.py:151
  163.8 3.8 all-to-all-start.3
  168.1 4.5 %all-to-all-done.3 = bf16[4,128,128]{2,1,0:T(8,128)(2,1)S(1)} async-done(((bf16[4,128,128]{2,1,0:T(8,128)(2,1)}), bf16[4,128,128]{2,1,0:T(8,128)(2,1)S(1)}, u32[]{:S(2)}, u32[]{:S(2)}) %all-to-all-start.3) | async-done | bytes 131104 | tf_op jit(solution)/shard_map/all_to_all | solution.py:156
  172.9 1.3 convolution_add_fusion
  174.2 0.7 all-gather.21.cloned.1.call-update
  175.0 0.7 all-gather.23.cloned.1.call-update
  175.7 10.7 %all-reduce = f32[8]{0:T(128)S(1)} all-reduce(f32[8]{0:T(128)S(1)} %get-tuple-element.181), channel_id=2, replica_groups=mesh['sp'=4,'fs'=4,'tp'=2] {'sp'}, use_global_device_ids=true, to_apply=%add | all-reduce | flops 8 | bytes 64
  187.2 14.7 %all_gather.45 = f32[1,2,256,256]{3,2,1,0:T(8,128)S(1)} all-gather(f32[1,2,64,256]{3,2,1,0:T(8,128)S(1)} %copy-done.4), channel_id=1, replica_groups=mesh['sp'=4,'fs'=4,'tp'=2] {'sp'}, dimensions={2}, use_global_device_ids=true | all-gather | bytes 655360 | tf_op jit(solution)/shard_map/all_gather | solution.py:193
  201.9 3.7 convolution_convert_fusion.3
  205.6 0.8 copy.52
  206.4 3.3 all-to-all-start.1
  209.8 1.3 minimum_convert_fusion
  211.1 3.7 all-to-all-done.1
  214.9 3.1 collective-permute-start
  218.7 0.7 convolution_add_fusion.2
  219.8 1.1 fusion.14
  221.7 14.9 %all-gather.25.cloned.1.call-done = f32[8,256,256]{2,1,0:T(8,128)} async-done(((f32[2,256,256]{2,1,0:T(8,128)}), f32[8,256,256]{2,1,0:T(8,128)}) %all-gather.25.cloned.1.call-update) | async-done | bytes 2097168 | tf_op jit(solution)/shard_map/all_gather | solution.py:27
  236.6 3.6 while.9
  236.6 1.2 fusion.67
  237.8 1.2 fusion.67
  239.0 1.2 fusion.67
  240.2 1.2 multiply_reduce_fusion
  241.5 83.7 %all-gather.21.cloned.1.call-done = bf16[512,4096]{1,0:T(8,128)(2,1)} async-done(((bf16[512,256]{1,0:T(8,128)(2,1)}), bf16[512,4096]{1,0:T(8,128)(2,1)}) %all-gather.21.cloned.1.call-update) | async-done | bytes 4194320 | tf_op jit(solution)/shard_map/all_gather | solution.py:209
  325.2 87.7 %all-gather.23.cloned.1.call-done = bf16[512,4096]{1,0:T(8,128)(2,1)} async-done(((bf16[512,256]{1,0:T(8,128)(2,1)}), bf16[512,4096]{1,0:T(8,128)(2,1)}) %all-gather.23.cloned.1.call-update) | async-done | bytes 4194320 | tf_op jit(solution)/shard_map/all_gather | solution.py:210
  412.9 5.8 %fusion.5 = bf16[128,4096]{1,0:T(8,128)(2,1)} fusion(bf16[512,4096]{1,0:T(8,128)(2,1)} %all-gather.23.cloned.1.call-done, bf16[512,4096]{1,0:T(8,128)(2,1)} %all-gather.21.cloned.1.call-done, bf16[128,512]{1,0:T(8,128)(2,1)S(1)} %copy.76, bf16[128,512]{1,0:T(8,128)(2,1)S(1)} %fusion.15), kind=kOutput, calls=%fused_computation.7 | convolution fusion | flops 1091567616 | bytes 9699328 | tf_op jit(solution)/shard_map/dot_general | solution.py:215
  418.8 6.7 %reduce-scatter.2.cloned.1.call-done = bf16[64,4096]{1,0:T(8,128)(2,1)} async-done(((bf16[128,4096]{1,0:T(8,128)(2,1)}), bf16[64,4096]{1,0:T(8,128)(2,1)}) %reduce-scatter.2.cloned.1.call-update) | async-done | bytes 524304 | tf_op jit(solution)/shard_map/reduce_scatter | solution.py:214
  (84 shorter events, 5.6 us)
Async XLA Ops:
  6.5 214.6 %copy-start = (bf16[4,256,256]{2,1,0:T(8,128)(2,1)S(1)}, bf16[4,256,256]{2,1,0:T(8,128)(2,1)}, u32[]{:S(2)}) copy-start(bf16[4,256,256]{2,1,0:T(8,128)(2,1)} %param.23) | copy-start | bytes 1572868
  6.5 17.1 %copy-start.1 = (bf16[256,512]{1,0:T(8,128)(2,1)S(1)}, bf16[256,512]{1,0:T(8,128)(2,1)}, u32[]{:S(2)}) copy-start(bf16[256,512]{1,0:T(8,128)(2,1)} %param.21) | copy-start | bytes 786436
  6.5 26.2 %copy-start.2 = (bf16[256,512]{1,0:T(8,128)(2,1)S(1)}, bf16[256,512]{1,0:T(8,128)(2,1)}, u32[]{:S(2)}) copy-start(bf16[256,512]{1,0:T(8,128)(2,1)} %param.22) | copy-start | bytes 786436
  6.5 45.9 %all-gather.17.cloned.1.call-start = ((), (), s32[]{:S(2)}) async-start(), calls=%async_computation.12 | async-start | bytes 1310720 | tf_op jit(solution)/shard_map/all_gather | solution.py:146
  19.3 22.6 %copy-start.3 = (bf16[256,512]{1,0:T(8,128)(2,1)S(1)}, bf16[256,512]{1,0:T(8,128)(2,1)}, u32[]{:S(2)}) copy-start(bf16[256,512]{1,0:T(8,128)(2,1)} %param.19) | copy-start | bytes 786436
  19.3 81.7 %all-gather.11.cloned.1.call-start = ((), (), s32[]{:S(2)}) async-start(), calls=%async_computation.9 | async-start | bytes 5242880 | tf_op jit(solution)/shard_map/all_gather | solution.py:137
  20.9 25.3 %copy-start.8 = (u32[32]{0:T(128)S(1)}, u32[32]{0:T(128)}, u32[]{:S(2)}) copy-start(u32[32]{0:T(128)} %constant.104) | copy-start | bytes 388
  20.9 26.6 %copy-start.5 = (f32[2]{0:T(128)S(1)}, f32[2]{0:T(128)}, u32[]{:S(2)}) copy-start(f32[2]{0:T(128)} %param.25) | copy-start | bytes 28
  23.5 107.0 %all-gather.19.cloned.1.call-start = ((), (), s32[]{:S(2)}) async-start(), calls=%async_computation.13 | async-start | bytes 1310720 | tf_op jit(solution)/shard_map/all_gather | solution.py:147
  32.7 126.7 %all-gather.15.cloned.1.call-start = ((), (), s32[]{:S(2)}) async-start(), calls=%async_computation.11 | async-start | bytes 1310720 | tf_op jit(solution)/shard_map/all_gather | solution.py:148
  42.8 8.8 %all-to-all-start = ((bf16[256,4,128]{0,2,1:T(8,128)(2,1)}), bf16[256,4,128]{0,2,1:T(8,128)(2,1)S(1)}, u32[]{:S(2)}, u32[]{:S(2)}) async-start(bf16[256,4,128]{0,2,1:T(8,128)(2,1)} %bitcast.2), calls=%async_computation | async-start | bytes 524288 | tf_op jit(solution)/shard_map/all_to_all | solution.py:139
  46.2 155.7 %all-gather.13.cloned.1.call-start = ((), (), s32[]{:S(2)}) async-start(), calls=%async_computation.10 | async-start | bytes 1310720 | tf_op jit(solution)/shard_map/all_gather | solution.py:145
  105.5 29.6 %all-to-all-start.5 = ((bf16[4,128,128]{1,2,0:T(8,128)(2,1)}), bf16[4,128,128]{1,2,0:T(8,128)(2,1)S(1)}, u32[]{:S(2)}, u32[]{:S(2)}) async-start(bf16[4,128,128]{1,2,0:T(8,128)(2,1)} %copy.60), calls=%async_computation.5 | async-start | bytes 262144 | tf_op jit(solution)/shard_map/all_to_all | solution.py:156
  135.1 28.7 %all-to-all-start.7 = ((bf16[4,128,128]{1,2,0:T(8,128)(2,1)}), bf16[4,128,128]{1,2,0:T(8,128)(2,1)S(1)}, u32[]{:S(2)}, u32[]{:S(2)}) async-start(bf16[4,128,128]{1,2,0:T(8,128)(2,1)} %copy.65), calls=%async_computation.7 | async-start | bytes 262144 | tf_op jit(solution)/shard_map/all_to_all | solution.py:156
  163.8 22.6 %copy-start.7 = (f32[1024]{0:T(1024)S(1)}, f32[1024]{0:T(1024)}, u32[]{:S(2)}) copy-start(f32[1024]{0:T(1024)} %param.24) | copy-start | bytes 12292
  163.8 22.7 %copy-start.6 = (s32[4]{0:T(128)S(1)}, s32[4]{0:T(128)}, u32[]{:S(2)}) copy-start(s32[4]{0:T(128)} %constant.99.clone) | copy-start | bytes 52
  163.8 23.4 %copy-start.4 = (f32[1,2,64,256]{3,2,1,0:T(8,128)S(1)}, f32[1,2,64,256]{3,2,1,0:T(8,128)}, u32[]{:S(2)}) copy-start(f32[1,2,64,256]{3,2,1,0:T(8,128)} %param.26) | copy-start | bytes 393220
  163.8 8.8 %all-to-all-start.3 = ((bf16[4,128,128]{2,1,0:T(8,128)(2,1)}), bf16[4,128,128]{2,1,0:T(8,128)(2,1)S(1)}, u32[]{:S(2)}, u32[]{:S(2)}) async-start(bf16[4,128,128]{2,1,0:T(8,128)(2,1)} %bitcast.22), calls=%async_computation.3 | async-start | bytes 262144 | tf_op jit(solution)/shard_map/all_to_all | solution.py:156
  167.6 69.0 %all-gather.25.cloned.1.call-start = ((), (), s32[]{:S(2)}) async-start(), calls=%async_computation.17 | async-start | bytes 2621440 | tf_op jit(solution)/shard_map/all_gather | solution.py:27
  174.2 151.0 %all-gather.21.cloned.1.call-start = ((), (), s32[]{:S(2)}) async-start(), calls=%async_computation.14 | async-start | bytes 4456448 | tf_op jit(solution)/shard_map/all_gather | solution.py:209
  174.9 238.0 %all-gather.23.cloned.1.call-start = ((), (), s32[]{:S(2)}) async-start(), calls=%async_computation.15 | async-start | bytes 4456448 | tf_op jit(solution)/shard_map/all_gather | solution.py:210
  206.4 8.3 %all-to-all-start.1 = ((bf16[4,128,128]{1,2,0:T(8,128)(2,1)}), bf16[4,128,128]{1,2,0:T(8,128)(2,1)S(1)}, u32[]{:S(2)}, u32[]{:S(2)}) async-start(bf16[4,128,128]{1,2,0:T(8,128)(2,1)} %copy.52), calls=%async_computation.1 | async-start | bytes 262144 | tf_op jit(solution)/shard_map/all_to_all | solution.py:156
  209.7 215.7 %reduce-scatter.2.cloned.1.call-start = ((), (), s32[]{:S(2)}) async-start(), calls=%async_computation.16 | async-start | bytes 1572864 | tf_op jit(solution)/shard_map/reduce_scatter | solution.py:214
  214.9 4.6 %collective-permute-start = (bf16[16,512]{1,0:T(8,128)(2,1)S(1)}, bf16[16,512]{1,0:T(8,128)(2,1)S(1)}, u32[]{:S(2)}, u32[]{:S(2)}) collective-permute-start(bf16[16,512]{1,0:T(8,128)(2,1)S(1)} %copy.75), channel_id=1, source_target_pairs={{0,8},{8,16},{16,24},{1,9},{9,17},{17,25},{2,10},{10,18},{18,26},{... | collective-permute-start | bytes 49160 | tf_op jit(solution)/shard_map/ppermute | solution.py:22
Sparse Core Ops, SparseCore 0:
  19.4 27.6 all-gather.16
  49.0 51.9 all-gather.10
  102.6 27.9 all-gather.18
  132.0 27.3 all-gather.14
  160.8 28.7 all-gather.12
  191.1 45.4 all-gather.24
  239.3 85.8 all-gather.20
  327.9 84.9 all-gather.22
  418.9 6.5 reduce-scatter.1
where the time goes:
time: 433 us; the launch traced here: 432 us
  waiting for transfers between devices  297 us (69%)
  blocking collectives  52.3 us (12%)
  matrix products  25.7 us (6%)
  starting transfers between devices  20.9 us (5%)
  between operations  14.2 us (3%)
  other arithmetic  11.1 us (3%)
  local copies, waits for them, and re-layouts  10.4 us (2%)
    all_gather x1, waiting for transfers between devices, on_device(): lax.all_gather(retention_back, ('sp', 'fs'), axis=1, tiled=True)  87.7 us
    all_gather x1, waiting for transfers between devices, on_device(): lax.all_gather(pool_back, ('sp', 'fs'), axis=1, tiled=True)  83.7 us
    all_gather x1, waiting for transfers between devices, on_device(): group_normed = lax.all_gather(normed, 'fs', axis=0, tiled=True)  48.6 us
    all_gather x1, waiting for transfers between devices, on_device(): lax.all_gather(quarters[2], 'sp', axis=0, tiled=True)  21.8 us
    all_gather x1, waiting for transfers between devices, on_device(): lax.all_gather(quarters[3], 'sp', axis=0, tiled=True)  20.7 us
    dot_general x4, matrix products, on_device(): jnp.dot(group_normed, piece_w, preferred_element_type=jnp.float32)  15.6 us
    all_gather x1, waiting for transfers between devices, carried_in(): pieces = jax.tree.map(lambda part: lax.all_gather(part, axis), value)  14.9 us
    all_gather x1, blocking collectives, on_device(): whole_start = lax.all_gather(start_state, 'sp', axis=2, tiled=True)[0]  14.7 us
  transfers between devices with their start and end apart: 15, of which 11 were waited for; matrix products, arithmetic and copies ran while one was open for 9% of the time, Pallas kernels for 0%

commit v1 on v0

--- a/solution.py
+++ b/solution.py
@@ -10,6 +10,11 @@
 rope_base = 10000.0
 highest_precision = lax.Precision.HIGHEST
 window_list = (2, 4, 8, 16)
+
+
+def gathered_along(x, name, along):
+    blocks = lax.all_gather(x, name)
+    return jnp.concatenate(blocks, axis=along)
 
 
 def shortened(x):
@@ -207,7 +212,7 @@
     ret_out = retained_output.reshape(length, head_count * head_dim).astype(jnp.bfloat16)
     pool_cols, retention_cols = (
         lax.all_gather(pool_back, ("sp", "fs"), axis=1, tiled=True),
-        lax.all_gather(retention_back, ("sp", "fs"), axis=1, tiled=True),
+        gathered_along(retention_back, ("sp", "fs"), 1),
     )
     weight_local = jnp.concatenate([pool_cols, retention_cols], axis=0)
     joined = jnp.concatenate([pool_out, ret_out], axis=1)

time: 433 us -> 423 us (0.977)
  waiting for transfers between devices: 297 us -> 279 us
  blocking collectives: 52.3 us -> 60.6 us
  starting transfers between devices: 20.9 us -> 15.9 us
    all_gather x1, waiting for transfers between devices: 87.7 us -> 48.7 us  [gathered_along(): blocks = lax.all_gather(x, name)]
    all_gather x1, waiting for transfers between devices: 14.9 us -> 41.1 us  [carried_in(): pieces = jax.tree.map(lambda part: lax.all_gather(part, axis), value)]
    all_to_all x0 -> x1, blocking collectives: none -> 8.11 us  [on_device(): lax.all_to_all(pool_proj, 'fs', split_axis=1, concat_axis=0, tiled=True)]
    reshape x0 -> x1, local copies, waits for them, and re-layouts: none -> 4.76 us  [gathered_along(): return jnp.concatenate(blocks, axis=along)]
  transfers between devices with their start and end apart: 15 -> 14, of which waited for: 11 -> 9; matrix products, arithmetic and copies ran while one was open for 9% -> 10% of each run, Pallas kernels for 0% -> 0%
where the time goes in v1:
time: 423 us; the launch traced here: 422 us
  waiting for transfers between devices  279 us (66%)
  blocking collectives  60.6 us (14%)
  matrix products  25.8 us (6%)
  starting transfers between devices  15.9 us (4%)
  local copies, waits for them, and re-layouts  14.6 us (3%)
  between operations  14.3 us (3%)
  other arithmetic  11.1 us (3%)
    all_gather x1, waiting for transfers between devices, on_device(): lax.all_gather(pool_back, ('sp', 'fs'), axis=1, tiled=True)  83.4 us
    all_gather x1, waiting for transfers between devices, gathered_along(): blocks = lax.all_gather(x, name)  48.7 us
    all_gather x1, waiting for transfers between devices, on_device(): group_normed = lax.all_gather(normed, 'fs', axis=0, tiled=True)  47.3 us
    all_gather x1, waiting for transfers between devices, carried_in(): pieces = jax.tree.map(lambda part: lax.all_gather(part, axis), value)  41.1 us
    all_gather x1, waiting for transfers between devices, on_device(): lax.all_gather(quarters[2], 'sp', axis=0, tiled=True)  21.8 us
    all_gather x1, waiting for transfers between devices, on_device(): lax.all_gather(quarters[3], 'sp', axis=0, tiled=True)  20.7 us
    dot_general x4, matrix products, on_device(): jnp.dot(group_normed, piece_w, preferred_element_type=jnp.float32)  15.7 us
    all_gather x1, blocking collectives, on_device(): whole_start = lax.all_gather(start_state, 'sp', axis=2, tiled=True)[0]  14.9 us
  transfers between devices with their start and end apart: 14, of which 9 were waited for; matrix products, arithmetic and copies ran while one was open for 10% of the time, Pallas kernels for 0%

profile of v1, /device:TPU:0, one launch (start us, length us, event | category | flops | bytes accessed | tf_op | source)
XLA Modules:
  0.0 421.5 jit_solution(11480839695405417434)
XLA Ops:
  6.5 1.2 copy.61
  7.7 10.7 %all_to_all.137 = bf16[256,4,128]{0,2,1:T(8,128)(2,1)S(1)} all-to-all(bf16[256,4,128]{0,2,1:T(8,128)(2,1)S(1)} %bitcast.107), channel_id=1, replica_groups=mesh['sp'=4,'fs'=4,'tp'=2] {'fs'}, dimensions={1} | all-to-all | bytes 524288 | tf_op jit(solution)/shard_map/all_to_all | solution.py:145
  18.4 0.9 copy.62
  19.4 1.5 fusion.8
  20.9 2.6 fusion.10
  23.7 8.1 %all_to_all.138 = bf16[256,4,128]{0,2,1:T(8,128)(2,1)S(1)} all-to-all(bf16[256,4,128]{0,2,1:T(8,128)(2,1)S(1)} %bitcast.108), channel_id=1, replica_groups=mesh['sp'=4,'fs'=4,'tp'=2] {'fs'}, dimensions={1} | all-to-all | bytes 524288 | tf_op jit(solution)/shard_map/all_to_all | solution.py:146
  31.9 0.8 copy.67
  32.9 8.1 %all_to_all.139 = bf16[256,4,128]{0,2,1:T(8,128)(2,1)S(1)} all-to-all(bf16[256,4,128]{0,2,1:T(8,128)(2,1)S(1)} %bitcast.109), channel_id=1, replica_groups=mesh['sp'=4,'fs'=4,'tp'=2] {'fs'}, dimensions={1} | all-to-all | bytes 524288 | tf_op jit(solution)/shard_map/all_to_all | solution.py:147
  41.0 0.8 copy.59
  42.1 8.1 %all_to_all.140 = bf16[256,4,128]{0,2,1:T(8,128)(2,1)S(1)} all-to-all(bf16[256,4,128]{0,2,1:T(8,128)(2,1)S(1)} %bitcast.110), channel_id=1, replica_groups=mesh['sp'=4,'fs'=4,'tp'=2] {'fs'}, dimensions={1} | all-to-all | bytes 524288 | tf_op jit(solution)/shard_map/all_to_all | solution.py:144
  50.2 0.9 copy.54
  51.7 0.7 dynamic-slice.2
  53.7 47.3 %all-gather.12.cloned.1.call-done = bf16[512,4096]{1,0:T(8,128)(2,1)} async-done(((bf16[128,4096]{1,0:T(8,128)(2,1)}), bf16[512,4096]{1,0:T(8,128)(2,1)}) %all-gather.12.cloned.1.call-update) | async-done | bytes 4194320 | tf_op jit(solution)/shard_map/all_gather | solution.py:142
  101.0 3.7 convolution_convert_fusion.1
  104.7 0.8 copy.63
  105.5 3.3 all-to-all-start.5
  108.8 21.8 %all-gather.20.cloned.1.call-done = bf16[4096,128]{1,0:T(8,128)(2,1)} async-done(((bf16[1024,128]{1,0:T(8,128)(2,1)}), bf16[4096,128]{1,0:T(8,128)(2,1)}) %all-gather.20.cloned.1.call-update) | async-done | bytes 1048592 | tf_op jit(solution)/shard_map/all_gather | solution.py:152
  130.6 3.7 convolution_convert_fusion
  134.3 0.8 copy.68
  135.1 3.6 all-to-all-start.7
  138.8 20.7 %all-gather.16.cloned.1.call-done = bf16[4096,128]{1,0:T(8,128)(2,1)} async-done(((bf16[1024,128]{1,0:T(8,128)(2,1)}), bf16[4096,128]{1,0:T(8,128)(2,1)}) %all-gather.16.cloned.1.call-update) | async-done | bytes 1048592 | tf_op jit(solution)/shard_map/all_gather | solution.py:153
  159.4 4.4 %convolution_convert_fusion.2 = bf16[512,128]{1,0:T(8,128)(2,1)} fusion(bf16[512,4096]{1,0:T(8,128)(2,1)} %all-gather.12.cloned.1.call-done, bf16[4096,128]{1,0:T(8,128)(2,1)} %all-gather.16.cloned.1.call-done), kind=kOutput, calls=%fused_computation.19 | convolution fusion | flops 536936448 | bytes 5373952 | tf_op jit(solution)/shard_map/dot_general | solution.py:156
  163.8 3.8 all-to-all-start.3
  168.1 4.5 %all-to-all-done.3 = bf16[4,128,128]{2,1,0:T(8,128)(2,1)S(1)} async-done(((bf16[4,128,128]{2,1,0:T(8,128)(2,1)}), bf16[4,128,128]{2,1,0:T(8,128)(2,1)S(1)}, u32[]{:S(2)}, u32[]{:S(2)}) %all-to-all-start.3) | async-done | bytes 131104 | tf_op jit(solution)/shard_map/all_to_all | solution.py:161
  172.9 1.3 convolution_add_fusion
  174.2 0.7 all-gather.22.cloned.1.call-update
  174.9 10.7 %all-reduce = f32[8]{0:T(128)S(1)} all-reduce(f32[8]{0:T(128)S(1)} %get-tuple-element.181), channel_id=2, replica_groups=mesh['sp'=4,'fs'=4,'tp'=2] {'sp'}, use_global_device_ids=true, to_apply=%add | all-reduce | flops 8 | bytes 64
  185.8 0.7 fusion.53
  186.5 14.9 %all_gather.48 = f32[1,2,256,256]{3,2,1,0:T(8,128)S(1)} all-gather(f32[1,2,64,256]{3,2,1,0:T(8,128)S(1)} %copy-done.4), channel_id=1, replica_groups=mesh['sp'=4,'fs'=4,'tp'=2] {'sp'}, dimensions={2}, use_global_device_ids=true | all-gather | bytes 655360 | tf_op jit(solution)/shard_map/all_gather | solution.py:198
  201.4 3.8 convolution_convert_fusion.3
  205.2 0.8 copy.55
  206.0 3.3 all-to-all-start.1
  209.3 1.3 minimum_convert_fusion
  210.7 3.6 all-to-all-done.1
  214.5 1.5 collective-permute-start
  216.6 0.7 convolution_add_fusion.2
  217.6 1.1 fusion.14
  219.5 48.7 %all-gather.26.cloned.1.call-done = bf16[8192,256]{1,0:T(8,128)(2,1)} async-done(((bf16[512,256]{1,0:T(8,128)(2,1)}), bf16[8192,256]{1,0:T(8,128)(2,1)}) %all-gather.26.cloned.1.call-update) | async-done | bytes 4194320 | tf_op jit(solution)/shard_map/all_gather | solution.py:16
  268.2 4.8 %copy.85 = bf16[16,64,8,256]{3,2,0,1:T(8,128)(2,1)} copy(bf16[16,64,8,256]{3,2,1,0:T(8,128)(2,1)} %bitcast.90) | data formatting | bytes 8388608 | tf_op jit(solution)/shard_map/reshape | solution.py:17
  273.0 41.1 %all-gather.24.cloned.1.call-done = f32[8,256,256]{2,1,0:T(8,128)} async-done(((f32[2,256,256]{2,1,0:T(8,128)}), f32[8,256,256]{2,1,0:T(8,128)}) %all-gather.24.cloned.1.call-update) | async-done | bytes 2097168 | tf_op jit(solution)/shard_map/all_gather | solution.py:32
  314.1 3.6 while.9
  314.1 1.2 fusion.67
  315.3 1.2 fusion.67
  316.5 1.2 fusion.67
  317.7 1.2 multiply_reduce_fusion
  319.0 83.4 %all-gather.22.cloned.1.call-done = bf16[512,4096]{1,0:T(8,128)(2,1)} async-done(((bf16[512,256]{1,0:T(8,128)(2,1)}), bf16[512,4096]{1,0:T(8,128)(2,1)}) %all-gather.22.cloned.1.call-update) | async-done | bytes 4194320 | tf_op jit(solution)/shard_map/all_gather | solution.py:214
  402.4 5.8 %fusion.5 = bf16[128,4096]{1,0:T(8,128)(2,1)} fusion(bf16[512,4096]{1,0:T(8,128)(2,1)} %bitcast.91, bf16[512,4096]{1,0:T(8,128)(2,1)} %all-gather.22.cloned.1.call-done, bf16[128,512]{1,0:T(8,128)(2,1)S(1)} %copy.80, bf16[128,512]{1,0:T(8,128)(2,1)S(1)} %fusion.15), kind=kOutput, calls=%fused_computation.7 | convolution fusion | flops 1091567616 | bytes 9699328 | tf_op jit(solution)/shard_map/dot_general | solution.py:220
  408.3 6.7 %reduce-scatter.2.cloned.1.call-done = bf16[64,4096]{1,0:T(8,128)(2,1)} async-done(((bf16[128,4096]{1,0:T(8,128)(2,1)}), bf16[64,4096]{1,0:T(8,128)(2,1)}) %reduce-scatter.2.cloned.1.call-update) | async-done | bytes 524304 | tf_op jit(solution)/shard_map/reduce_scatter | solution.py:219
  (84 shorter events, 4.9 us)
Async XLA Ops:
  6.5 212.4 %copy-start = (bf16[4,256,256]{2,1,0:T(8,128)(2,1)S(1)}, bf16[4,256,256]{2,1,0:T(8,128)(2,1)}, u32[]{:S(2)}) copy-start(bf16[4,256,256]{2,1,0:T(8,128)(2,1)} %param.23) | copy-start | bytes 1572868
  6.5 17.1 %copy-start.1 = (bf16[256,512]{1,0:T(8,128)(2,1)S(1)}, bf16[256,512]{1,0:T(8,128)(2,1)}, u32[]{:S(2)}) copy-start(bf16[256,512]{1,0:T(8,128)(2,1)} %param.21) | copy-start | bytes 786436
  6.5 26.2 %copy-start.2 = (bf16[256,512]{1,0:T(8,128)(2,1)S(1)}, bf16[256,512]{1,0:T(8,128)(2,1)}, u32[]{:S(2)}) copy-start(bf16[256,512]{1,0:T(8,128)(2,1)} %param.22) | copy-start | bytes 786436
  6.5 47.1 %all-gather.18.cloned.1.call-start = ((), (), s32[]{:S(2)}) async-start(), calls=%async_computation.12 | async-start | bytes 1310720 | tf_op jit(solution)/shard_map/all_gather | solution.py:151
  19.3 22.7 %copy-start.3 = (bf16[256,512]{1,0:T(8,128)(2,1)S(1)}, bf16[256,512]{1,0:T(8,128)(2,1)}, u32[]{:S(2)}) copy-start(bf16[256,512]{1,0:T(8,128)(2,1)} %param.19) | copy-start | bytes 786436
  19.3 81.7 %all-gather.12.cloned.1.call-start = ((), (), s32[]{:S(2)}) async-start(), calls=%async_computation.9 | async-start | bytes 5242880 | tf_op jit(solution)/shard_map/all_gather | solution.py:142
  20.9 30.8 %copy-start.8 = (u32[32]{0:T(128)S(1)}, u32[32]{0:T(128)}, u32[]{:S(2)}) copy-start(u32[32]{0:T(128)} %constant.104) | copy-start | bytes 388
  20.9 32.2 %copy-start.5 = (f32[2]{0:T(128)S(1)}, f32[2]{0:T(128)}, u32[]{:S(2)}) copy-start(f32[2]{0:T(128)} %param.25) | copy-start | bytes 28
  23.5 107.0 %all-gather.20.cloned.1.call-start = ((), (), s32[]{:S(2)}) async-start(), calls=%async_computation.13 | async-start | bytes 1310720 | tf_op jit(solution)/shard_map/all_gather | solution.py:152
  32.7 126.7 %all-gather.16.cloned.1.call-start = ((), (), s32[]{:S(2)}) async-start(), calls=%async_computation.11 | async-start | bytes 1310720 | tf_op jit(solution)/shard_map/all_gather | solution.py:153
  41.9 159.5 %all-gather.14.cloned.1.call-start = ((), (), s32[]{:S(2)}) async-start(), calls=%async_computation.10 | async-start | bytes 1310720 | tf_op jit(solution)/shard_map/all_gather | solution.py:150
  51.1 217.2 %all-gather.26.cloned.1.call-start = ((), (), s32[]{:S(2)}) async-start(), calls=%async_computation.17 | async-start | bytes 4456448 | tf_op jit(solution)/shard_map/all_gather | solution.py:16
  105.5 29.6 %all-to-all-start.5 = ((bf16[4,128,128]{1,2,0:T(8,128)(2,1)}), bf16[4,128,128]{1,2,0:T(8,128)(2,1)S(1)}, u32[]{:S(2)}, u32[]{:S(2)}) async-start(bf16[4,128,128]{1,2,0:T(8,128)(2,1)} %copy.63), calls=%async_computation.5 | async-start | bytes 262144 | tf_op jit(solution)/shard_map/all_to_all | solution.py:161
  135.1 28.7 %all-to-all-start.7 = ((bf16[4,128,128]{1,2,0:T(8,128)(2,1)}), bf16[4,128,128]{1,2,0:T(8,128)(2,1)S(1)}, u32[]{:S(2)}, u32[]{:S(2)}) async-start(bf16[4,128,128]{1,2,0:T(8,128)(2,1)} %copy.68), calls=%async_computation.7 | async-start | bytes 262144 | tf_op jit(solution)/shard_map/all_to_all | solution.py:161
  163.8 21.9 %copy-start.7 = (f32[1024]{0:T(1024)S(1)}, f32[1024]{0:T(1024)}, u32[]{:S(2)}) copy-start(f32[1024]{0:T(1024)} %param.24) | copy-start | bytes 12292
  163.8 22.0 %copy-start.6 = (s32[4]{0:T(128)S(1)}, s32[4]{0:T(128)}, u32[]{:S(2)}) copy-start(s32[4]{0:T(128)} %constant.99.clone) | copy-start | bytes 52
  163.8 22.7 %copy-start.4 = (f32[1,2,64,256]{3,2,1,0:T(8,128)S(1)}, f32[1,2,64,256]{3,2,1,0:T(8,128)}, u32[]{:S(2)}) copy-start(f32[1,2,64,256]{3,2,1,0:T(8,128)} %param.26) | copy-start | bytes 393220
  163.8 8.8 %all-to-all-start.3 = ((bf16[4,128,128]{2,1,0:T(8,128)(2,1)}), bf16[4,128,128]{2,1,0:T(8,128)(2,1)S(1)}, u32[]{:S(2)}, u32[]{:S(2)}) async-start(bf16[4,128,128]{2,1,0:T(8,128)(2,1)} %bitcast.22), calls=%async_computation.3 | async-start | bytes 262144 | tf_op jit(solution)/shard_map/all_to_all | solution.py:161
  167.6 146.5 %all-gather.24.cloned.1.call-start = ((), (), s32[]{:S(2)}) async-start(), calls=%async_computation.16 | async-start | bytes 2621440 | tf_op jit(solution)/shard_map/all_gather | solution.py:32
  174.2 228.3 %all-gather.22.cloned.1.call-start = ((), (), s32[]{:S(2)}) async-start(), calls=%async_computation.14 | async-start | bytes 4456448 | tf_op jit(solution)/shard_map/all_gather | solution.py:214
  206.0 8.3 %all-to-all-start.1 = ((bf16[4,128,128]{1,2,0:T(8,128)(2,1)}), bf16[4,128,128]{1,2,0:T(8,128)(2,1)S(1)}, u32[]{:S(2)}, u32[]{:S(2)}) async-start(bf16[4,128,128]{1,2,0:T(8,128)(2,1)} %copy.55), calls=%async_computation.1 | async-start | bytes 262144 | tf_op jit(solution)/shard_map/all_to_all | solution.py:161
  209.3 205.7 %reduce-scatter.2.cloned.1.call-start = ((), (), s32[]{:S(2)}) async-start(), calls=%async_computation.15 | async-start | bytes 1572864 | tf_op jit(solution)/shard_map/reduce_scatter | solution.py:219
  214.5 2.8 collective-permute-start
Sparse Core Ops, SparseCore 0:
  19.4 27.6 all-gather.17
  49.0 51.9 all-gather.11
  102.6 27.9 all-gather.19
  132.0 27.3 all-gather.15
  160.8 29.0 all-gather.13
  192.5 75.6 all-gather.25
  269.8 44.2 all-gather.23
  316.8 85.5 all-gather.21
  408.4 6.5 reduce-scatter.1
